TPU v7x, 32 devices: a whole 2x2x4 slice. The times are simulated.
32 devices in a mesh: fs: 4 (over z), tp: 8 (over y, x, core).
Axes of the slice: x: 2, y: 2, z: 4, core: 2. Of those that a mesh axis runs over, the one named last changes fastest.
Arguments:
- tokens: bfloat16 [768, 2304], P('fs'), may hold values from -6 to 6
- gate_train: float32 [8, 2304, 2304], P(None, 'fs', 'tp'), may hold values from -0.125 to 0.125
- up_train: float32 [8, 2304, 2304], P(None, 'fs', 'tp'), may hold values from -0.125 to 0.125
- down_train: float32 [8, 2304, 2304], P(None, 'fs', 'tp'), may hold values from -0.125 to 0.125
- gain: float32 [2304], P('fs'), may hold values from 0.1 to 1.9
- routes: int32 [768, 2], P('fs'), may hold values from 0 to 7, all different within a row; in each aligned block of 192 rows (0 to 191, 192 to 383, ...) at most 72 rows name the same one
- route_weights: float32 [768, 2], P('fs'), may hold values from 0.1 to 1
Outputs:
- gate_new: bfloat16 [8, 2304, 2304], P('tp')
- up_new: bfloat16 [8, 2304, 2304], P('tp')
- down_new: bfloat16 [8, 2304, 2304], P('tp')
- mixed: bfloat16 [768, 2304], P('fs', 'tp')
Inputs may be any that keep to these rules, and one draw needn't show every extreme that they name: `routes`: each row names two different experts; in each aligned block of 192 rows at most 72 rows name one expert, a bound that some block reaches.
All inputs are finite; a program needn't handle non-finite values.
Results may differ from a plain program's by a relative error of at most 0.0095.
Values may be sent and summed in bfloat16 or wider, within the bound.
A program may use at most 128 MiB of HBM per device.

v0:
```python
import jax
import jax.numpy as jnp
from jax import lax
from jax.sharding import PartitionSpec as P

CAP = 72
norm_eps = 1e-06


def arrange(matrix, tp_count):
    experts, row_count, col_count = matrix.shape
    slices = tp_count // experts
    piece_width = col_count // slices
    shaped = matrix.reshape(experts, row_count, slices, piece_width)
    return shaped.transpose(0, 2, 3, 1).reshape(tp_count, piece_width, row_count)


def shards(tokens, gate_train, up_train, down_train, gain, routes, route_weights):
    tp_count = lax.axis_size("tp")
    experts = gate_train.shape[0]
    slices = tp_count // experts
    gain_column = gain[None, :, None]
    gate_round = (gate_train * gain_column).astype(jnp.bfloat16)
    up_round = (up_train * gain_column).astype(jnp.bfloat16)
    down_round = down_train.astype(jnp.bfloat16)
    moved = (
        lax.all_to_all(
            arrange(gate_round, tp_count), "tp", split_axis=0, concat_axis=1, tiled=True
        ),
        lax.all_to_all(arrange(up_round, tp_count), "tp", split_axis=0, concat_axis=1, tiled=True),
        lax.all_to_all(
            arrange(down_round, tp_count), "tp", split_axis=0, concat_axis=1, tiled=True
        ),
    )
    tokens_wide = tokens.astype(jnp.float32)
    normed = (
        tokens_wide
        * lax.rsqrt(jnp.mean(tokens_wide * tokens_wide, axis=1, keepdims=True) + norm_eps)
    ).astype(jnp.bfloat16)
    expert = lax.axis_index("tp") // slices
    matches = routes == expert
    member = jnp.any(matches, axis=1)
    slot_index = jnp.cumsum(member.astype(jnp.int32)) - 1
    marked = jnp.where(member, slot_index, -1)
    picker = (marked[None, :] == jnp.arange(CAP, dtype=jnp.int32)[:, None]).astype(jnp.bfloat16)
    chosen = jnp.dot(picker, normed, preferred_element_type=jnp.float32).astype(jnp.bfloat16)
    contract_last = (((1,), (1,)), ((), ()))
    gate_new, up_new, down_new = (
        lax.all_gather(moved[0], "fs", axis=2, tiled=True),
        lax.all_gather(moved[1], "fs", axis=2, tiled=True),
        lax.all_gather(moved[2], "fs", axis=2, tiled=True),
    )
    gate_pre = lax.dot_general(
        chosen, gate_new[0], contract_last, preferred_element_type=jnp.float32
    )
    up_pre = lax.dot_general(chosen, up_new[0], contract_last, preferred_element_type=jnp.float32)
    hidden = (jax.nn.silu(gate_pre) * up_pre).astype(jnp.bfloat16)
    partial_value = jnp.dot(hidden, down_new[0], preferred_element_type=jnp.float32).astype(
        jnp.bfloat16
    )
    labels = jnp.arange(experts, dtype=jnp.int32)
    member_all = jnp.any(routes[:, :, None] == labels[None, None, :], axis=1)
    slots_all = jnp.cumsum(member_all.astype(jnp.int32), axis=0) - 1
    slot_pair = jnp.take_along_axis(slots_all, routes, axis=1)
    flat_index = slot_pair * experts + routes
    received = lax.all_to_all(
        partial_value.reshape(CAP, tp_count, -1), "tp", split_axis=1, concat_axis=1, tiled=True
    )
    summed = jnp.sum(received.reshape(CAP, experts, slices, -1).astype(jnp.float32), axis=2)
    summed = summed.reshape(CAP * experts, -1)
    picked = jnp.take(summed, flat_index, axis=0)
    mixed = jnp.sum(route_weights[:, :, None] * picked, axis=1)
    return (gate_new, up_new, down_new, mixed.astype(jnp.bfloat16))


def solution(mesh):
    in_specs = (
        P("fs", None),
        P(None, "fs", "tp"),
        P(None, "fs", "tp"),
        P(None, "fs", "tp"),
        P("fs"),
        P("fs", None),
        P("fs", None),
    )
    out_specs = (P("tp", None, None), P("tp", None, None), P("tp", None, None), P("fs", "tp"))
    return jax.shard_map(shards, mesh=mesh, in_specs=in_specs, out_specs=out_specs, check_vma=False)
```

profile of v0, /device:TPU:1, one launch (start us, length us, event | category | flops | bytes accessed | tf_op | source)
XLA Modules:
  0.0 690.3 jit_solution(4470130244694976679)
XLA Ops:
  7.2 0.0 all-gather.4.cloned.1.call-start
  7.2 5.4 fusion.16
  12.6 40.1 %all_to_all.41 = bf16[8,288,576]{2,1,0:T(8,128)(2,1)} all-to-all(bf16[8,288,576]{2,1,0:T(8,128)(2,1)S(1)} %get-tuple-element.23), channel_id=1, replica_groups=mesh['fs'=4,'tp'=8] {'tp'}, dimensions={0} | all-to-all | bytes 5308416 | tf_op jit(solution)/shard_map/all_to_all | solution.py:27
  52.6 4.5 copy.89
  57.1 0.0 all-gather.4.cloned.1.call-update
  57.1 0.0 all-gather.6.cloned.1.call-start
  57.2 39.1 %all_to_all.42 = bf16[8,288,576]{2,1,0:T(8,128)(2,1)} all-to-all(bf16[8,288,576]{2,1,0:T(8,128)(2,1)S(1)} %get-tuple-element.22), channel_id=1, replica_groups=mesh['fs'=4,'tp'=8] {'tp'}, dimensions={0} | all-to-all | bytes 5308416 | tf_op jit(solution)/shard_map/all_to_all | solution.py:30
  96.3 4.5 copy.90
  100.8 0.0 all-gather.6.cloned.1.call-update
  100.8 0.0 all-gather.8.cloned.1.call-start
  100.9 3.0 convert_bitcast_fusion
  103.9 0.0 copy-start.1
  103.9 38.2 %all_to_all.43 = bf16[8,288,576]{2,1,0:T(8,128)(2,1)S(1)} all-to-all(bf16[8,288,576]{2,1,0:T(8,128)(2,1)S(1)} %convert_bitcast_fusion), channel_id=1, replica_groups=mesh['fs'=4,'tp'=8] {'tp'}, dimensions={0} | all-to-all | bytes 5308416 | tf_op jit(solution)/shard_map/all_to_all | solution.py:31
  142.2 3.4 copy.91
  145.5 0.0 all-gather.8.cloned.1.call-update
  145.6 0.0 copy-done.1
  145.6 0.6 reduce-window.15
  146.2 0.2 slice_reduce_fusion
  146.5 0.1 copy.93
  146.6 0.1 reshape.127
  146.7 0.1 add_bitcast_fusion
  146.8 0.0 copy-start
  146.8 2.7 gather_fusion.1
  149.5 0.1 reshape.130
  149.6 0.1 copy.94
  149.8 0.3 reduce-window.19
  150.1 0.1 slice.22
  150.2 0.1 slice_reduce_fusion.1
  150.3 0.0 copy-done
  150.3 0.3 fusion.17
  150.6 0.1 add_bitcast_fusion.1
  150.6 0.4 convolution_convert_fusion
  151.0 91.9 %all-gather.4.cloned.1.call-done = bf16[1,2304,2304]{1,2,0:T(8,128)(2,1)} async-done(((bf16[1,2304,576]{1,2,0:T(8,128)(2,1)}), bf16[1,2304,2304]{1,2,0:T(8,128)(2,1)}) %all-gather.4.cloned.1.call-update) | async-done | bytes 10616848 | tf_op jit(solution)/shard_map/all_gather | solution.py:49
  242.9 6.0 fusion.4
  248.9 0.0 copy-start.2
  249.0 180.4 %all-gather.6.cloned.1.call-done = bf16[1,2304,2304]{1,2,0:T(8,128)(2,1)} async-done(((bf16[1,2304,576]{1,2,0:T(8,128)(2,1)}), bf16[1,2304,2304]{1,2,0:T(8,128)(2,1)}) %all-gather.6.cloned.1.call-update) | async-done | bytes 10616848 | tf_op jit(solution)/shard_map/all_gather | solution.py:50
  429.4 186.4 %all-gather.8.cloned.1.call-done = bf16[1,2304,2304]{1,2,0:T(8,128)(2,1)} async-done(((bf16[1,2304,576]{1,2,0:T(8,128)(2,1)}), bf16[1,2304,2304]{1,2,0:T(8,128)(2,1)}) %all-gather.8.cloned.1.call-update) | async-done | bytes 10616848 | tf_op jit(solution)/shard_map/all_gather | solution.py:51
  615.8 11.9 %fusion.12 = bf16[72,2304]{1,0:T(8,128)(2,1)S(1)} fusion(bf16[1,2304,2304]{1,2,0:T(8,128)(2,1)} %all-gather.8.cloned.1.call-done, bf16[72,2304]{1,0:T(8,128)(2,1)S(1)} %convolution_convert_fusion, bf16[1,2304,2304]{1,2,0:T(8,128)(2,1)} %all-gather.6.cloned.1.call-done, f32[72,2304]{1,0:T(8,128)S(1)} %fusion.4), kind=kOutput, calls=%fused_computation.12 | convolution fusion | flops 1529985024 | bytes 22560768 | tf_op jit(solution)/shard_map/dot_general | solution.py:58
  627.7 0.7 reshape.112
  628.4 0.8 copy.96
  629.2 4.2 all-to-all-start.3
  633.3 0.1 copy.98
  633.5 0.1 reshape.121
  633.6 0.2 copy.95
  633.8 0.0 copy-done.2
  633.8 0.1 copy.92
  633.9 15.2 %copy.100 = bf16[1,2304,2304]{2,1,0:T(8,128)(2,1)} copy(bf16[1,2304,2304]{1,2,0:T(8,128)(2,1)} %all-gather.6.cloned.1.call-done) | data formatting | bytes 21233664
  649.1 15.2 %copy.99 = bf16[1,2304,2304]{2,1,0:T(8,128)(2,1)} copy(bf16[1,2304,2304]{1,2,0:T(8,128)(2,1)} %all-gather.4.cloned.1.call-done) | data formatting | bytes 21233664
  664.4 15.2 %copy.101 = bf16[1,2304,2304]{2,1,0:T(8,128)(2,1)} copy(bf16[1,2304,2304]{1,2,0:T(8,128)(2,1)} %all-gather.8.cloned.1.call-done) | data formatting | bytes 21233664
  679.6 0.0 all-to-all-done.3
  679.6 0.1 copy.103
  679.6 1.7 gather_fusion
  681.4 0.3 reshape.120
  681.7 2.0 multiply_reduce_fusion
  (12 shorter events, 0.2 us)
Async XLA Ops:
  7.2 235.8 %all-gather.4.cloned.1.call-start = ((), (), s32[]{:S(2)}) async-start(), calls=%async_computation.4 | async-start | bytes 13271040 | tf_op jit(solution)/shard_map/all_gather | solution.py:49
  57.1 372.2 %all-gather.6.cloned.1.call-start = ((), (), s32[]{:S(2)}) async-start(), calls=%async_computation.5 | async-start | bytes 13271040 | tf_op jit(solution)/shard_map/all_gather | solution.py:50
  100.8 514.9 %all-gather.8.cloned.1.call-start = ((), (), s32[]{:S(2)}) async-start(), calls=%async_computation.6 | async-start | bytes 13271040 | tf_op jit(solution)/shard_map/all_gather | solution.py:51
  103.9 41.7 %copy-start.1 = (s32[192,2]{0,1:T(2,128)S(1)}, s32[192,2]{0,1:T(2,128)}, u32[]{:S(2)}) copy-start(s32[192,2]{0,1:T(2,128)} %param.12) | copy-start | bytes 4612
  146.8 3.5 copy-start
  248.9 384.8 %copy-start.2 = (f32[192,2]{0,1:T(2,128)S(1)}, f32[192,2]{0,1:T(2,128)}, u32[]{:S(2)}) copy-start(f32[192,2]{0,1:T(2,128)} %param.13) | copy-start | bytes 4612
  629.2 50.4 %all-to-all-start.3 = ((bf16[72,8,288]{2,0,1:T(8,128)(2,1)}), bf16[72,8,288]{2,0,1:T(8,128)(2,1)S(1)}, u32[]{:S(2)}, u32[]{:S(2)}) async-start(bf16[72,8,288]{2,0,1:T(8,128)(2,1)} %copy.96), calls=%async_computation.3 | async-start | bytes 884736 | tf_op jit(solution)/shard_map/all_to_all | solution.py:66
Sparse Core Ops, SparseCore 0:
  57.3 185.6 all-gather.3
  245.1 184.2 all-gather.5
  431.5 184.2 all-gather.7
where the time goes:
time: 692 us; the launch traced here: 690 us
  waiting for transfers between devices  459 us (66%)
  blocking collectives  117 us (17%)
  local copies, waits for them, and re-layouts  65.7 us (9%)
  matrix products  18.3 us (3%)
  between operations  13.9 us (2%)
  other arithmetic  11.9 us (2%)
    all_gather x1, waiting for transfers between devices, shards(): lax.all_gather(moved[2], 'fs', axis=2, tiled=True)  186 us
    all_gather x1, waiting for transfers between devices, shards(): lax.all_gather(moved[1], 'fs', axis=2, tiled=True)  180 us
    all_gather x1, waiting for transfers between devices, shards(): lax.all_gather(moved[0], 'fs', axis=2, tiled=True)  91.9 us
    unnamed x10, local copies, waits for them, and re-layouts  45.8 us
    all_to_all x1, blocking collectives, shards(): lax.all_to_all(arrange(gate_round, tp_count), 'tp', split_axis=0, concat_...  40.1 us
    all_to_all x1, blocking collectives, shards(): lax.all_to_all(arrange(up_round, tp_count), 'tp', split_axis=0, concat_ax...  39.1 us
    all_to_all x1, blocking collectives, shards(): lax.all_to_all(arrange(down_round, tp_count), 'tp', split_axis=0, concat_...  38.2 us
  transfers between devices with their start and end apart: 4, of which 3 were waited for; matrix products, arithmetic and copies ran while one was open for 10% of the time, Pallas kernels for 0%

commit v1 on v0

--- a/solution.py
+++ b/solution.py
@@ -45,8 +45,13 @@
     picker = (marked[None, :] == jnp.arange(CAP, dtype=jnp.int32)[:, None]).astype(jnp.bfloat16)
     chosen = jnp.dot(picker, normed, preferred_element_type=jnp.float32).astype(jnp.bfloat16)
     contract_last = (((1,), (1,)), ((), ()))
+
+    def test_the_works(vals):
+        view_out = jnp.concatenate(lax.all_gather(vals, axis_name="fs"), 2)
+        return view_out
+
     gate_new, up_new, down_new = (
-        lax.all_gather(moved[0], "fs", axis=2, tiled=True),
+        test_the_works(moved[0]),
         lax.all_gather(moved[1], "fs", axis=2, tiled=True),
         lax.all_gather(moved[2], "fs", axis=2, tiled=True),
     )

time: 692 us -> 692 us (level)
  no operation moved by 1% of the time
where the time goes in v1:
time: 692 us; the launch traced here: 690 us
  waiting for transfers between devices  459 us (66%)
  blocking collectives  117 us (17%)
  local copies, waits for them, and re-layouts  65.7 us (9%)
  matrix products  18.3 us (3%)
  between operations  13.9 us (2%)
  other arithmetic  11.9 us (2%)
    all_gather x1, waiting for transfers between devices, shards(): lax.all_gather(moved[2], 'fs', axis=2, tiled=True)  186 us
    all_gather x1, waiting for transfers between devices, shards(): lax.all_gather(moved[1], 'fs', axis=2, tiled=True)  180 us
    all_gather x1, waiting for transfers between devices, test_the_works(): view_out = jnp.concatenate(lax.all_gather(vals, axis_name='fs'), 2)  91.9 us
    unnamed x10, local copies, waits for them, and re-layouts  45.8 us
    all_to_all x1, blocking collectives, shards(): lax.all_to_all(arrange(gate_round, tp_count), 'tp', split_axis=0, concat_...  40.1 us
    all_to_all x1, blocking collectives, shards(): lax.all_to_all(arrange(up_round, tp_count), 'tp', split_axis=0, concat_ax...  39.1 us
    all_to_all x1, blocking collectives, shards(): lax.all_to_all(arrange(down_round, tp_count), 'tp', split_axis=0, concat_...  38.2 us
  transfers between devices with their start and end apart: 4, of which 3 were waited for; matrix products, arithmetic and copies ran while one was open for 10% of the time, Pallas kernels for 0%

profile of v1, /device:TPU:1, one launch (start us, length us, event | category | flops | bytes accessed | tf_op | source)
XLA Modules:
  0.0 690.3 jit_solution(12122676894567847487)
XLA Ops:
  7.2 0.0 all-gather.4.cloned.1.call-start
  7.2 5.4 fusion.14
  12.6 40.1 %all_to_all.38 = bf16[8,288,576]{2,1,0:T(8,128)(2,1)} all-to-all(bf16[8,288,576]{2,1,0:T(8,128)(2,1)S(1)} %get-tuple-element.31), channel_id=1, replica_groups=mesh['fs'=4,'tp'=8] {'tp'}, dimensions={0} | all-to-all | bytes 5308416 | tf_op jit(solution)/shard_map/all_to_all | solution.py:27
  52.6 4.5 copy.111
  57.1 0.0 all-gather.4.cloned.1.call-update
  57.1 0.0 all-gather.6.cloned.1.call-start
  57.2 39.1 %all_to_all.39 = bf16[8,288,576]{2,1,0:T(8,128)(2,1)} all-to-all(bf16[8,288,576]{2,1,0:T(8,128)(2,1)S(1)} %get-tuple-element.30), channel_id=1, replica_groups=mesh['fs'=4,'tp'=8] {'tp'}, dimensions={0} | all-to-all | bytes 5308416 | tf_op jit(solution)/shard_map/all_to_all | solution.py:30
  96.3 4.5 copy.113
  100.8 0.0 all-gather.6.cloned.1.call-update
  100.8 0.0 all-gather.8.cloned.1.call-start
  100.9 3.0 convert_bitcast_fusion
  103.9 0.0 copy-start.1
  103.9 38.2 %all_to_all.40 = bf16[8,288,576]{2,1,0:T(8,128)(2,1)S(1)} all-to-all(bf16[8,288,576]{2,1,0:T(8,128)(2,1)S(1)} %convert_bitcast_fusion), channel_id=1, replica_groups=mesh['fs'=4,'tp'=8] {'tp'}, dimensions={0} | all-to-all | bytes 5308416 | tf_op jit(solution)/shard_map/all_to_all | solution.py:31
  142.2 3.4 copy.114
  145.5 0.0 all-gather.8.cloned.1.call-update
  145.6 0.0 copy-done.1
  145.6 0.6 reduce-window.15
  146.2 0.2 slice_reduce_fusion
  146.5 0.1 copy.116
  146.6 0.1 reshape.136
  146.7 0.1 add_bitcast_fusion
  146.8 0.0 copy-start
  146.8 2.7 gather_fusion.1
  149.5 0.1 reshape.139
  149.6 0.1 copy.117
  149.8 0.3 reduce-window.19
  150.1 0.1 slice.22
  150.2 0.1 slice_reduce_fusion.1
  150.3 0.0 copy-done
  150.3 0.3 fusion.15
  150.6 0.1 add_bitcast_fusion.1
  150.6 0.4 convolution_convert_fusion
  151.0 91.9 %all-gather.4.cloned.1.call-done = bf16[4,1,2304,576]{2,3,1,0:T(8,128)(2,1)} async-done(((bf16[1,1,2304,576]{2,3,1,0:T(8,128)(2,1)}), bf16[4,1,2304,576]{2,3,1,0:T(8,128)(2,1)}) %all-gather.4.cloned.1.call-update) | async-done | bytes 10616848 | tf_op jit(solution)/shard_map/all_gather | solution.py:50
  242.9 6.0 fusion.28
  248.9 0.0 copy-start.2
  249.0 180.4 %all-gather.6.cloned.1.call-done = bf16[1,2304,2304]{1,2,0:T(8,128)(2,1)} async-done(((bf16[1,2304,576]{1,2,0:T(8,128)(2,1)}), bf16[1,2304,2304]{1,2,0:T(8,128)(2,1)}) %all-gather.6.cloned.1.call-update) | async-done | bytes 10616848 | tf_op jit(solution)/shard_map/all_gather | solution.py:55
  429.4 186.4 %all-gather.8.cloned.1.call-done = bf16[1,2304,2304]{1,2,0:T(8,128)(2,1)} async-done(((bf16[1,2304,576]{1,2,0:T(8,128)(2,1)}), bf16[1,2304,2304]{1,2,0:T(8,128)(2,1)}) %all-gather.8.cloned.1.call-update) | async-done | bytes 10616848 | tf_op jit(solution)/shard_map/all_gather | solution.py:56
  615.8 11.9 %fusion.10 = bf16[72,2304]{1,0:T(8,128)(2,1)S(1)} fusion(bf16[1,2304,2304]{1,2,0:T(8,128)(2,1)} %all-gather.8.cloned.1.call-done, bf16[72,2304]{1,0:T(8,128)(2,1)S(1)} %convolution_convert_fusion, bf16[1,2304,2304]{1,2,0:T(8,128)(2,1)} %all-gather.6.cloned.1.call-done, f32[72,2304]{1,0:T(8,128)S(1)} %fusion.28), kind=kOutput, calls=%fused_computation.10 | convolution fusion | flops 1529985024 | bytes 22560768 | tf_op jit(solution)/shard_map/dot_general | solution.py:63
  627.7 0.7 reshape.121
  628.4 0.8 copy.119
  629.2 4.2 all-to-all-start.3
  633.3 0.1 copy.121
  633.5 0.1 reshape.130
  633.6 0.2 copy.118
  633.8 0.0 copy-done.2
  633.8 0.1 copy.115
  633.9 15.2 %copy.122 = bf16[1,2304,2304]{2,1,0:T(8,128)(2,1)} copy(bf16[1,2304,2304]{1,2,0:T(8,128)(2,1)} %bitcast.64) | data formatting | bytes 21233664
  649.1 15.2 %copy.123 = bf16[1,2304,2304]{2,1,0:T(8,128)(2,1)} copy(bf16[1,2304,2304]{1,2,0:T(8,128)(2,1)} %all-gather.6.cloned.1.call-done) | data formatting | bytes 21233664
  664.4 15.2 %copy.124 = bf16[1,2304,2304]{2,1,0:T(8,128)(2,1)} copy(bf16[1,2304,2304]{1,2,0:T(8,128)(2,1)} %all-gather.8.cloned.1.call-done) | data formatting | bytes 21233664
  679.6 0.0 all-to-all-done.3
  679.6 0.1 copy.126
  679.6 1.7 gather_fusion
  681.4 0.3 reshape.129
  681.7 2.0 multiply_reduce_fusion
  (12 shorter events, 0.2 us)
Async XLA Ops:
  7.2 235.8 %all-gather.4.cloned.1.call-start = ((), (), s32[]{:S(2)}) async-start(), calls=%async_computation.4 | async-start | bytes 13271040 | tf_op jit(solution)/shard_map/all_gather | solution.py:50
  57.1 372.2 %all-gather.6.cloned.1.call-start = ((), (), s32[]{:S(2)}) async-start(), calls=%async_computation.5 | async-start | bytes 13271040 | tf_op jit(solution)/shard_map/all_gather | solution.py:55
  100.8 514.9 %all-gather.8.cloned.1.call-start = ((), (), s32[]{:S(2)}) async-start(), calls=%async_computation.6 | async-start | bytes 13271040 | tf_op jit(solution)/shard_map/all_gather | solution.py:56
  103.9 41.7 %copy-start.1 = (s32[192,2]{0,1:T(2,128)S(1)}, s32[192,2]{0,1:T(2,128)}, u32[]{:S(2)}) copy-start(s32[192,2]{0,1:T(2,128)} %param.12) | copy-start | bytes 4612
  146.8 3.5 copy-start
  248.9 384.8 %copy-start.2 = (f32[192,2]{0,1:T(2,128)S(1)}, f32[192,2]{0,1:T(2,128)}, u32[]{:S(2)}) copy-start(f32[192,2]{0,1:T(2,128)} %param.13) | copy-start | bytes 4612
  629.2 50.4 %all-to-all-start.3 = ((bf16[72,8,288]{2,0,1:T(8,128)(2,1)}), bf16[72,8,288]{2,0,1:T(8,128)(2,1)S(1)}, u32[]{:S(2)}, u32[]{:S(2)}) async-start(bf16[72,8,288]{2,0,1:T(8,128)(2,1)} %copy.119), calls=%async_computation.3 | async-start | bytes 884736 | tf_op jit(solution)/shard_map/all_to_all | solution.py:71
Sparse Core Ops, SparseCore 0:
  57.3 185.6 all-gather.3
  245.1 184.2 all-gather.5
  431.5 184.2 all-gather.7
